TPU v7x, 32 devices: a whole 2x2x4 slice. The times are simulated.
32 devices in a mesh: sp: 4 (over y, x), tp: 8 (over z, core).
Axes of the slice: x: 2, y: 2, z: 4, core: 2. Of those that a mesh axis runs over, the one named last changes fastest.
Arguments:
- upstream: bfloat16 [1024, 4096], P('sp', 'tp'), may hold values from -6 to 6
- stream: bfloat16 [1024, 4096], P('sp', 'tp'), may hold values from -400 to 400
- norm_gain: float32 [4096], P('tp'), may hold values from 0.1 to 1.9
- routes: int32 [1024, 2], P('sp'), may hold values from 0 to 3, all different within a row; in each aligned block of 256 rows (0 to 255, 256 to 511, ...) at most 192 rows name the same one
- route_weights: float32 [1024, 2], P('sp'), may hold values from 0.1 to 1
- w_gate: bfloat16 [4, 4096, 2048], P('sp', None, 'tp'), may hold values from -0.09375 to 0.09375
- w_up: bfloat16 [4, 4096, 2048], P('sp', None, 'tp'), may hold values from -0.09375 to 0.09375
- w_down: bfloat16 [4, 2048, 4096], P('sp', 'tp'), may hold values from -0.125 to 0.125
- value_in: bfloat16 [1024, 2048], P('sp', 'tp'), may hold values from -6 to 6
- gate_in: bfloat16 [1024, 2048], P('sp', 'tp'), may hold values from -6 to 6
- conv_pre: bfloat16 [1024, 2048], P('sp', 'tp'), may hold values from -200 to 200
- ln_gain: float32 [2048], P('tp'), may hold values from 0.1 to 1.9
- conv_taps: float32 [31, 2048], P(None, 'tp'), may hold values from -1 to 1
- w_out: bfloat16 [2048, 4096], P('tp'), may hold values from -0.125 to 0.125
Outputs:
- grad_gate: float32 [4, 4096, 2048], P('sp', None, 'tp')
- grad_up: float32 [4, 4096, 2048], P('sp', None, 'tp')
- grad_down: float32 [4, 2048, 4096], P('sp', 'tp')
- grad_out: float32 [2048, 4096], P('tp', 'sp')
- value_grad: bfloat16 [1024, 2048], P('sp', 'tp')
- gate_grad: bfloat16 [1024, 2048], P('sp', 'tp')
Inputs may be any that keep to these rules, and one draw needn't show every extreme that they name: `routes`: each token names two different experts. Among the tokens of one index of sp no expert is named more than 192 times, and in every draw some expert exactly 192 times.
All inputs are finite; a program needn't handle non-finite values.
Results may differ from a plain program's by a relative error of at most 0.0071.
Values may be sent and summed in bfloat16 or wider, within the bound.
A program may use at most 128 MiB of HBM per device.

v0:
```python
import jax
import jax.numpy as jnp
from jax import lax
from jax.sharding import PartitionSpec as P

EPSILON = 1e-06


def shifted(block, axis, distance):
    devices = range(lax.axis_size(axis))
    route = [(i - distance, i) for i in devices if i - distance in devices]
    return lax.ppermute(block, axis, route)


def silu_slope(values):
    logistic = jax.nn.sigmoid(values)
    return logistic * (1.0 + values * (1.0 - logistic))


def per_device(
    upstream,
    stream,
    norm_gain,
    routes,
    route_weights,
    w_gate,
    w_up,
    w_down,
    value_in,
    gate_in,
    conv_pre,
    ln_gain,
    conv_taps,
    w_out,
):
    tok_rows, width_part = stream.shape
    token_groups = lax.axis_size("sp")
    width_groups = lax.axis_size("tp")
    model_width = width_part * width_groups
    channels = conv_pre.shape[1] * width_groups
    tap_count = conv_taps.shape[0]
    capacity = 3 * tok_rows // token_groups
    experts = w_gate.shape[0] * token_groups
    slot_count = experts * capacity
    expert_rows = token_groups * capacity
    residual = stream.astype(jnp.float32)
    conv_vals = conv_pre.astype(jnp.float32)
    row_squares, conv_total, conv_squares = lax.psum(
        (
            jnp.sum(residual * residual, axis=1),
            jnp.sum(conv_vals, axis=1),
            jnp.sum(conv_vals * conv_vals, axis=1),
        ),
        "tp",
    )
    inverse = lax.rsqrt(row_squares / model_width + EPSILON)[:, None]
    normed = (norm_gain[None, :] * residual * inverse).astype(jnp.bfloat16)
    flat_experts = routes.reshape(-1)
    one_hot = (flat_experts[:, None] == jnp.arange(experts, dtype=jnp.int32)[None, :]).astype(
        jnp.int32
    )
    slot_rank = jnp.sum((jnp.cumsum(one_hot, axis=0) - one_hot) * one_hot, axis=1)
    slot_index = (flat_experts * capacity + slot_rank).reshape(tok_rows, 2)
    slot_ids = jnp.arange(slot_count, dtype=jnp.int32)[:, None]
    first_hit = slot_ids == slot_index[None, :, 0]
    second_hit = slot_ids == slot_index[None, :, 1]
    any_hit = jnp.logical_or(first_hit, second_hit)
    picker = any_hit.astype(jnp.bfloat16)
    slot_weight = jnp.sum(
        jnp.where(first_hit, route_weights[None, :, 0], 0.0)
        + jnp.where(second_hit, route_weights[None, :, 1], 0.0),
        axis=1,
    )
    token_iota = jnp.arange(tok_rows, dtype=jnp.int32)[None, :]
    slot_token = jnp.where(
        jnp.any(any_hit, axis=1), jnp.sum(jnp.where(any_hit, token_iota, 0), axis=1), tok_rows
    )
    columns = normed.shape[1]
    normed_pad = jnp.concatenate([normed, jnp.zeros((1, columns), jnp.bfloat16)], axis=0)
    upstream_pad = jnp.concatenate([upstream, jnp.zeros((1, columns), jnp.bfloat16)], axis=0)
    inputs = normed_pad[slot_token]
    cotangent = (upstream_pad[slot_token].astype(jnp.float32) * slot_weight[:, None]).astype(
        jnp.bfloat16
    )
    sent_inputs = inputs.reshape(experts, capacity, columns)
    sent_cotangent = cotangent.reshape(experts, capacity, columns)
    part_inputs, part_cotangent = (
        lax.all_to_all(sent_inputs, "sp", split_axis=0, concat_axis=0, tiled=True),
        lax.all_to_all(sent_cotangent, "sp", split_axis=0, concat_axis=0, tiled=True),
    )
    inputs, cotangent = (
        lax.all_gather(part_inputs.reshape(expert_rows, width_part), "tp", axis=1, tiled=True),
        lax.all_gather(part_cotangent.reshape(expert_rows, width_part), "tp", axis=1, tiled=True),
    )
    gate_mat = w_gate[0]
    upper_mat = w_up[0]
    down_mat = w_down[0]
    gate_pre = jnp.dot(inputs, gate_mat, preferred_element_type=jnp.float32)
    upper_pre = jnp.dot(inputs, upper_mat, preferred_element_type=jnp.float32)
    active = (jax.nn.silu(gate_pre) * upper_pre).astype(jnp.bfloat16)
    active_back = lax.dot_general(
        cotangent, down_mat, (((1,), (1,)), ((), ())), preferred_element_type=jnp.float32
    )
    gate_back = (active_back * upper_pre * silu_slope(gate_pre)).astype(jnp.bfloat16)
    upper_back = (active_back * jax.nn.silu(gate_pre)).astype(jnp.bfloat16)
    grad_gate = lax.dot_general(
        inputs, gate_back, (((0,), (0,)), ((), ())), preferred_element_type=jnp.float32
    )
    grad_up = lax.dot_general(
        inputs, upper_back, (((0,), (0,)), ((), ())), preferred_element_type=jnp.float32
    )
    grad_down = lax.dot_general(
        active, cotangent, (((0,), (0,)), ((), ())), preferred_element_type=jnp.float32
    )
    input_part = lax.dot_general(
        gate_back, gate_mat, (((1,), (1,)), ((), ())), preferred_element_type=jnp.float32
    ) + lax.dot_general(
        upper_back, upper_mat, (((1,), (1,)), ((), ())), preferred_element_type=jnp.float32
    )
    input_back = lax.psum_scatter(input_part, "tp", scatter_dimension=1, tiled=True).astype(
        jnp.bfloat16
    )
    returned = lax.all_to_all(
        input_back.reshape(token_groups, capacity, width_part),
        "sp",
        split_axis=0,
        concat_axis=0,
        tiled=True,
    )
    returned = returned.reshape(slot_count, width_part)
    token_back = lax.dot_general(
        picker, returned, (((0,), (0,)), ((), ())), preferred_element_type=jnp.float32
    )
    gained = norm_gain[None, :] * token_back
    inner_sum = lax.psum(jnp.sum(gained * residual, axis=1), "tp")
    norm_back = inverse * gained - residual * inverse**3 * (inner_sum / model_width)[:, None]
    stream_grad = (upstream.astype(jnp.float32) + norm_back).astype(jnp.bfloat16)
    full_grad = lax.all_gather(stream_grad, "tp", axis=1, tiled=True)
    mean_val = (conv_total / channels)[:, None]
    variance = (conv_squares / channels)[:, None] - mean_val * mean_val
    inv_std = lax.rsqrt(variance + EPSILON)
    centred = (conv_vals - mean_val) * inv_std
    scaled = centred * ln_gain[None, :]
    mixed_out = jax.nn.silu(scaled).astype(jnp.bfloat16)
    columns = full_grad
    grad_rows = lax.psum_scatter(
        lax.dot_general(
            columns, mixed_out, (((0,), (0,)), ((), ())), preferred_element_type=jnp.float32
        ),
        "sp",
        scatter_dimension=0,
        tiled=True,
    )
    grad_out = grad_rows.T
    mixed_back = lax.dot_general(
        full_grad, w_out, (((1,), (1,)), ((), ())), preferred_element_type=jnp.float32
    )
    norm_in = mixed_back * silu_slope(scaled) * ln_gain[None, :]
    norm_total, norm_cross = lax.psum(
        (jnp.sum(norm_in, axis=1), jnp.sum(norm_in * centred, axis=1)), "tp"
    )
    conv_back = inv_std * (
        norm_in - (norm_total / channels)[:, None] - centred * (norm_cross / channels)[:, None]
    )
    next_rim = shifted(conv_back[: tap_count - 1], "sp", -1)
    padded = jnp.concatenate([conv_back, next_rim], axis=0)
    glu_back = jnp.zeros(conv_back.shape, jnp.float32)
    for tap_index in range(tap_count):
        offset = tap_count - 1 - tap_index
        glu_back = glu_back + conv_taps[tap_index][None, :] * padded[offset : offset + tok_rows]
    gate_sigma = jax.nn.sigmoid(gate_in.astype(jnp.float32))
    value_grad = (glu_back * gate_sigma).astype(jnp.bfloat16)
    gate_grad = (glu_back * value_in.astype(jnp.float32) * gate_sigma * (1.0 - gate_sigma)).astype(
        jnp.bfloat16
    )
    return (grad_gate[None], grad_up[None], grad_down[None], grad_out, value_grad, gate_grad)


def solution(mesh):
    return jax.shard_map(
        per_device,
        mesh=mesh,
        in_specs=(
            P("sp", "tp"),
            P("sp", "tp"),
            P("tp"),
            P("sp", None),
            P("sp", None),
            P("sp", None, "tp"),
            P("sp", None, "tp"),
            P("sp", "tp", None),
            P("sp", "tp"),
            P("sp", "tp"),
            P("sp", "tp"),
            P("tp"),
            P(None, "tp"),
            P("tp", None),
        ),
        out_specs=(
            P("sp", None, "tp"),
            P("sp", None, "tp"),
            P("sp", "tp", None),
            P("tp", "sp"),
            P("sp", "tp"),
            P("sp", "tp"),
        ),
        check_vma=False,
    )
```

profile of v0, /device:TPU:0, one launch (start us, length us, event | category | flops | bytes accessed | tf_op | source)
XLA Modules:
  0.0 439.3 jit_solution(1147835568961126519)
XLA Ops:
  7.2 0.0 copy-start
  7.2 0.0 all-gather.4.cloned.1.call-start
  7.2 0.9 copy.36
  8.2 0.1 eq.60
  8.3 0.1 eq.56
  8.5 1.2 reduce-window.6
  9.7 0.2 slice_reduce_fusion
  9.9 0.2 reduce-window.9
  10.1 0.1 add_bitcast_fusion
  10.2 0.1 reduce_sum.85
  10.4 0.1 copy.38
  10.4 0.7 multiply_add_fusion
  11.1 0.2 fusion.22
  11.4 0.2 select_reduce_fusion
  11.6 1.1 fusion.15
  12.7 18.1 %psum.42 = f32[256]{0:T(256)S(1)} all-reduce(f32[256]{0:T(256)S(1)} %fusion.15), channel_id=1, replica_groups=mesh['sp'=4,'tp'=8] {'tp'}, use_global_device_ids=true, to_apply=%region_1.0 | all-reduce | flops 256 | bytes 2048 | tf_op jit(solution)/shard_map/psum | solution.py:48
  30.8 1.1 fusion.14
  31.9 2.7 gather_fusion
  34.6 12.2 %all_to_all.15 = bf16[4,192,512]{2,1,0:T(8,128)(2,1)} all-to-all(bf16[4,192,512]{2,1,0:T(8,128)(2,1)S(1)} %bitcast.98), channel_id=1, replica_groups=mesh['sp'=4,'tp'=8] {'sp'}, dimensions={0} | all-to-all | bytes 1572864 | tf_op jit(solution)/shard_map/all_to_all | solution.py:88
  46.8 0.0 all-gather.4.cloned.1.call-update
  46.8 0.0 all-gather.6.cloned.1.call-start
  46.9 2.7 gather_fusion.1
  49.6 0.2 add_reduce_fusion
  49.8 0.1 mul.483
  49.9 0.2 fusion.9
  50.1 11.6 %all_to_all.16 = bf16[4,192,512]{2,1,0:T(8,128)(2,1)} all-to-all(bf16[4,192,512]{2,1,0:T(8,128)(2,1)S(1)} %fusion.9), channel_id=1, replica_groups=mesh['sp'=4,'tp'=8] {'sp'}, dimensions={0} | all-to-all | bytes 1572864 | tf_op jit(solution)/shard_map/all_to_all | solution.py:89
  61.8 0.0 all-gather.6.cloned.1.call-update
  61.8 0.2 reduce-scatter.3.cloned.1.call-start
  62.1 47.4 %all-gather.4.cloned.1.call-done = bf16[768,4096]{1,0:T(8,128)(2,1)} async-done(((bf16[768,512]{1,0:T(8,128)(2,1)}), bf16[768,4096]{1,0:T(8,128)(2,1)}) %all-gather.4.cloned.1.call-update) | async-done | bytes 6291472 | tf_op jit(solution)/shard_map/all_gather | solution.py:92
  109.4 4.7 %fusion.2 = f32[768,256]{1,0:T(8,128)S(1)} fusion(bf16[768,4096]{1,0:T(8,128)(2,1)} %all-gather.4.cloned.1.call-done, bf16[1,4096,256]{2,1,0:T(8,128)(2,1)S(1)} %copy-done), kind=kOutput, calls=%fused_computation.37 | convolution fusion | flops 1610612736 | bytes 9175040 | tf_op jit(solution)/shard_map/dot_general | solution.py:98
  114.2 0.5 copy-done.18
  114.6 2.7 fusion.5
  117.3 57.1 %all-gather.6.cloned.1.call-done = bf16[768,4096]{1,0:T(8,128)(2,1)} async-done(((bf16[768,512]{1,0:T(8,128)(2,1)}), bf16[768,4096]{1,0:T(8,128)(2,1)}) %all-gather.6.cloned.1.call-update) | async-done | bytes 6291472 | tf_op jit(solution)/shard_map/all_gather | solution.py:93
  174.4 5.5 %multiply_convert_fusion.1 = (bf16[768,256]{1,0:T(8,128)(2,1)S(1)}, bf16[768,256]{1,0:T(8,128)(2,1)S(1)}) fusion(f32[768,256]{1,0:T(8,128)S(1)} %fusion.2, f32[768,256]{1,0:T(8,128)} %fusion.5, bf16[768,4096]{1,0:T(8,128)(2,1)} %all-gather.6.cloned.1.call-done, bf16[1,256,4096]{2,1,0:T(8,128)(2,1)} %param.21), kind=kOutput, calls=%fused_computation.54 | convolution fusion | flops 1613168640 | bytes 10747904 | tf_op jit(solution)/shard_map/dot_general | solution.py:101
  179.9 1.8 fusion
  181.8 6.4 %convolution_add_fusion = f32[768,4096]{1,0:T(8,128)} fusion(f32[768,4096]{1,0:T(8,128)S(1)} %fusion, bf16[768,256]{1,0:T(8,128)(2,1)S(1)} %get-tuple-element.47, bf16[1,4096,256]{2,1,0:T(8,128)(2,1)S(1)} %copy-done.5), kind=kOutput, calls=%fused_computation.2 | convolution fusion | flops 1613758464 | bytes 27656192 | tf_op jit(solution)/shard_map/dot_general | solution.py:117
  188.2 0.0 reduce-scatter.3.cloned.1.call-update
  188.2 0.0 copy-start.17
  188.3 127.9 %reduce-scatter.3.cloned.1.call-done = f32[768,512]{1,0:T(8,128)} async-done(((f32[768,4096]{1,0:T(8,128)}), f32[768,512]{1,0:T(8,128)}) %reduce-scatter.3.cloned.1.call-update) | async-done | bytes 1572880 | tf_op jit(solution)/shard_map/reduce_scatter | solution.py:120
  316.2 2.4 convert_element_type.72
  318.6 3.6 all-to-all-start.2
  322.2 0.1 convert_reduce_fusion
  322.4 8.9 %all-to-all-done.2 = bf16[4,192,512]{2,1,0:T(8,128)(2,1)S(1)} async-done(((bf16[4,192,512]{2,1,0:T(8,128)(2,1)}), bf16[4,192,512]{2,1,0:T(8,128)(2,1)S(1)}, u32[]{:S(2)}, u32[]{:S(2)}) %all-to-all-start.2) | async-done | bytes 786464 | tf_op jit(solution)/shard_map/all_to_all | solution.py:123
  331.3 0.5 fusion.20
  331.8 14.8 %all-reduce.3 = (f32[256]{0:T(256)S(1)}, f32[256]{0:T(256)S(1)}, f32[256]{0:T(256)S(1)}) all-reduce(f32[256]{0:T(256)S(1)} %get-tuple-element.88, f32[256]{0:T(256)S(1)} %get-tuple-element.39, f32[256]{0:T(256)S(1)} %get-tuple-element.38), channel_id=1, replica_groups=mesh['sp'=4,'tp'=8] {'tp'}, use_global_device_ids=true, to_apply=%region_10.11 | all-reduce | flops 768 | bytes 6144 | tf_op jit(solution)/shard_map/psum | solution.py:135
  346.6 0.9 fusion.19
  347.6 0.0 all-gather.8.cloned.1.call-update
  347.6 0.3 reduce-scatter.5.cloned.1.call-start
  347.9 25.8 %all-gather.8.cloned.1.call-done = bf16[256,4096]{1,0:T(8,128)(2,1)} async-done(((bf16[256,512]{1,0:T(8,128)(2,1)}), bf16[256,4096]{1,0:T(8,128)(2,1)}) %all-gather.8.cloned.1.call-update) | async-done | bytes 2097168 | tf_op jit(solution)/shard_map/all_gather | solution.py:138
  373.7 4.4 fusion.132
  378.1 0.0 reduce-scatter.5.cloned.1.call-update
  378.1 0.7 copy-done.14
  378.9 0.2 copy-done.12
  379.1 6.7 %convolution_bitcast_fusion.2 = f32[1,4096,256]{2,1,0:T(8,128)} fusion(bf16[768,4096]{1,0:T(8,128)(2,1)} %all-gather.4.cloned.1.call-done, bf16[768,256]{1,0:T(8,128)(2,1)S(1)} %copy-done.12), kind=kOutput, calls=%fused_computation.5 | convolution fusion | flops 1610612736 | bytes 10878976 | tf_op jit(solution)/shard_map/dot_general | solution.py:106
  385.8 6.9 %convolution_bitcast_fusion = f32[1,256,4096]{2,1,0:T(8,128)} fusion(bf16[768,4096]{1,0:T(8,128)(2,1)} %all-gather.6.cloned.1.call-done, f32[768,256]{1,0:T(8,128)S(1)} %copy-done.6, f32[768,256]{1,0:T(8,128)S(1)} %fusion.2), kind=kOutput, calls=%fused_computation.3 | convolution fusion | flops 1611792384 | bytes 12058624 | tf_op jit(solution)/shard_map/dot_general | solution.py:112
  392.7 0.9 fusion.145
  393.6 15.3 %all-reduce.2 = (f32[256]{0:T(256)S(1)}, f32[256]{0:T(256)S(1)}) all-reduce(f32[256]{0:T(256)S(1)} %get-tuple-element.37, f32[256]{0:T(256)S(1)} %get-tuple-element.36), channel_id=1, replica_groups=mesh['sp'=4,'tp'=8] {'tp'}, use_global_device_ids=true, to_apply=%region_19.20 | all-reduce | flops 512 | bytes 4096 | tf_op jit(solution)/shard_map/psum | solution.py:159
  408.9 0.2 fusion.128
  409.2 1.4 collective-permute-start
  410.6 6.8 %convolution_bitcast_fusion.1 = f32[1,4096,256]{2,1,0:T(8,128)} fusion(bf16[768,4096]{1,0:T(8,128)(2,1)} %all-gather.4.cloned.1.call-done, bf16[768,256]{1,0:T(8,128)(2,1)S(1)} %get-tuple-element.47), kind=kOutput, calls=%fused_computation.4 | convolution fusion | flops 1610612736 | bytes 10878976 | tf_op jit(solution)/shard_map/dot_general | solution.py:109
  417.4 2.1 multiply_convert_fusion.4
  419.5 0.7 multiply_convert_fusion.5
  420.2 10.0 %reduce-scatter.5.cloned.1.call-done = f32[1024,256]{1,0:T(8,128)} async-done(((f32[4096,256]{1,0:T(8,128)}), f32[1024,256]{1,0:T(8,128)}) %reduce-scatter.5.cloned.1.call-update) | async-done | bytes 1048592 | tf_op jit(solution)/shard_map/reduce_scatter | solution.py:146
  430.2 2.5 copy.39
  (53 shorter events, 0.3 us)
Async XLA Ops:
  7.2 102.2 %copy-start = (bf16[1,4096,256]{2,1,0:T(8,128)(2,1)S(1)}, bf16[1,4096,256]{2,1,0:T(8,128)(2,1)}, u32[]{:S(2)}) copy-start(bf16[1,4096,256]{2,1,0:T(8,128)(2,1)} %param.19) | copy-start | bytes 6291460
  7.2 102.2 %all-gather.4.cloned.1.call-start = ((), (), s32[]{:S(2)}) async-start(), calls=%async_computation.5 | async-start | bytes 7077888 | tf_op jit(solution)/shard_map/all_gather | solution.py:92
  31.9 14.9 %copy-start.8 = (bf16[256,512]{1,0:T(8,128)(2,1)S(1)}, bf16[256,512]{1,0:T(8,128)(2,1)}, u32[]{:S(2)}) copy-start(bf16[256,512]{1,0:T(8,128)(2,1)} %param.14) | copy-start | bytes 786436
  46.8 2.8 copy-start.16
  46.8 127.6 %all-gather.6.cloned.1.call-start = ((), (), s32[]{:S(2)}) async-start(), calls=%async_computation.6 | async-start | bytes 7077888 | tf_op jit(solution)/shard_map/all_gather | solution.py:93
  61.8 254.4 %reduce-scatter.3.cloned.1.call-start = ((), (), s32[]{:S(2)}) async-start(), calls=%async_computation.7 | async-start | bytes 14155776 | tf_op jit(solution)/shard_map/reduce_scatter | solution.py:120
  109.4 4.7 %copy-start.4 = (bf16[1,4096,256]{2,1,0:T(8,128)(2,1)S(1)}, bf16[1,4096,256]{2,1,0:T(8,128)(2,1)}, u32[]{:S(2)}) copy-start(bf16[1,4096,256]{2,1,0:T(8,128)(2,1)} %param.20) | copy-start | bytes 6291460
  109.4 5.2 %copy-start.18 = (bf16[768,4096]{1,0:T(8,128)(2,1)S(1)}, bf16[768,4096]{1,0:T(8,128)(2,1)}, u32[]{:S(2)}) copy-start(bf16[768,4096]{1,0:T(8,128)(2,1)} %all-gather.4.cloned.1.call-done) | copy-start | bytes 18874372
  179.9 1.9 copy-start.11
  179.9 1.9 copy-start.5
  188.2 134.0 %copy-start.7 = (bf16[256,256]{1,0:T(8,128)(2,1)S(1)}, bf16[256,256]{1,0:T(8,128)(2,1)}, u32[]{:S(2)}) copy-start(bf16[256,256]{1,0:T(8,128)(2,1)} %param.24) | copy-start | bytes 393220
  188.2 143.1 %copy-start.3 = (bf16[256,512]{1,0:T(8,128)(2,1)S(1)}, bf16[256,512]{1,0:T(8,128)(2,1)}, u32[]{:S(2)}) copy-start(bf16[256,512]{1,0:T(8,128)(2,1)} %param.15) | copy-start | bytes 786436
  188.2 143.1 %copy-start.15 = (f32[512]{0:T(512)S(1)}, f32[512]{0:T(512)}, u32[]{:S(2)}) copy-start(f32[512]{0:T(512)} %param.16) | copy-start | bytes 6148
  188.2 158.4 %copy-start.9 = (bf16[256,512]{1,0:T(8,128)(2,1)S(1)}, bf16[256,512]{1,0:T(8,128)(2,1)}, u32[]{:S(2)}) copy-start(bf16[256,512]{1,0:T(8,128)(2,1)} %param.14) | copy-start | bytes 786436
  188.2 185.5 %copy-start.17 = (f32[256]{0:T(256)S(1)}, f32[256]{0:T(256)}, u32[]{:S(2)}) copy-start(f32[256]{0:T(256)} %param.25) | copy-start | bytes 3076
  318.6 12.7 %all-to-all-start.2 = ((bf16[4,192,512]{2,1,0:T(8,128)(2,1)}), bf16[4,192,512]{2,1,0:T(8,128)(2,1)S(1)}, u32[]{:S(2)}, u32[]{:S(2)}) async-start(bf16[4,192,512]{2,1,0:T(8,128)(2,1)} %bitcast.15), calls=%async_computation.3 | async-start | bytes 1572864 | tf_op jit(solution)/shard_map/all_to_all | solution.py:123
  322.2 51.5 %all-gather.8.cloned.1.call-start = ((), (), s32[]{:S(2)}) async-start(), calls=%async_computation.8 | async-start | bytes 2359296 | tf_op jit(solution)/shard_map/all_gather | solution.py:138
  347.6 82.7 %reduce-scatter.5.cloned.1.call-start = ((), (), s32[]{:S(2)}) async-start(), calls=%async_computation.9 | async-start | bytes 5242880 | tf_op jit(solution)/shard_map/reduce_scatter | solution.py:146
  378.1 0.8 copy-start.14
  378.1 1.0 copy-start.12
  379.1 6.7 %copy-start.6 = (f32[768,256]{1,0:T(8,128)S(1)}, f32[768,256]{1,0:T(8,128)}, u32[]{:S(2)}) copy-start(f32[768,256]{1,0:T(8,128)} %fusion.5) | copy-start | bytes 2359300
  385.8 6.9 %copy-start.2 = (bf16[256,4096]{1,0:T(8,128)(2,1)S(1)}, bf16[256,4096]{1,0:T(8,128)(2,1)}, u32[]{:S(2)}) copy-start(bf16[256,4096]{1,0:T(8,128)(2,1)} %all-gather.8.cloned.1.call-done) | copy-start | bytes 6291460
  385.8 6.9 %copy-start.19 = (bf16[256,4096]{1,0:T(8,128)(2,1)S(1)}, bf16[256,4096]{1,0:T(8,128)(2,1)}, u32[]{:S(2)}) copy-start(bf16[256,4096]{1,0:T(8,128)(2,1)} %param.27) | copy-start | bytes 6291460
  409.2 8.3 %copy-start.10 = (bf16[256,256]{1,0:T(8,128)(2,1)S(1)}, bf16[256,256]{1,0:T(8,128)(2,1)}, u32[]{:S(2)}) copy-start(bf16[256,256]{1,0:T(8,128)(2,1)} %param.23) | copy-start | bytes 393220
  409.2 8.3 %copy-start.13 = (bf16[256,256]{1,0:T(8,128)(2,1)S(1)}, bf16[256,256]{1,0:T(8,128)(2,1)}, u32[]{:S(2)}) copy-start(bf16[256,256]{1,0:T(8,128)(2,1)} %param.22) | copy-start | bytes 393220
  409.2 8.2 %collective-permute-start = (f32[30,256]{1,0:T(8,128)S(1)}, f32[30,256]{1,0:T(8,128)S(1)}, u32[]{:S(2)}, u32[]{:S(2)}) collective-permute-start(f32[30,256]{1,0:T(8,128)S(1)} %slice.279), channel_id=1, source_target_pairs={{8,0},{16,8},{24,16},{9,1},{17,9},{25,17},{10,2},{18,10},{26,18},{... | collective-permute-start | bytes 92168 | tf_op jit(solution)/shard_map/ppermute | solution.py:12
  410.6 22.2 %copy-start.1 = (bf16[1,4096,256]{2,1,0:T(8,128)(2,1)S(1)}, bf16[1,4096,256]{2,1,0:T(8,128)(2,1)}, u32[]{:S(2)}) copy-start(bf16[1,4096,256]{2,1,0:T(8,128)(2,1)} %param.19) | copy-start | bytes 6291460
Sparse Core Ops, SparseCore 0:
  46.9 62.4 all-gather.3
  111.0 63.3 all-gather.5
  188.4 127.7 reduce-scatter.2
  347.7 25.9 all-gather.7
  378.2 51.9 reduce-scatter.4
where the time goes:
time: 440 us; the launch traced here: 439 us
  waiting for transfers between devices  277 us (63%)
  blocking collectives  72 us (16%)
  matrix products  47.3 us (11%)
  between operations  14.1 us (3%)
  other arithmetic  11.8 us (3%)
  local copies, waits for them, and re-layouts  11.2 us (3%)
  starting transfers between devices  5.63 us (1%)
    reduce_scatter x1, waiting for transfers between devices, per_device(): lax.psum_scatter(input_part, 'tp', scatter_dimension=1, tiled=True)  128 us
    all_gather x1, waiting for transfers between devices, per_device(): lax.all_gather(part_cotangent.reshape(expert_rows, width_part), 'tp', axi...  57.1 us
    all_gather x1, waiting for transfers between devices, per_device(): lax.all_gather(part_inputs.reshape(expert_rows, width_part), 'tp', axis=1...  47.4 us
    all_gather x1, waiting for transfers between devices, per_device(): full_grad = lax.all_gather(stream_grad, 'tp', axis=1, tiled=True)  25.8 us
    psum x1, blocking collectives, per_device(): lax.psum((jnp.sum(residual * residual, axis=1), jnp.sum(conv_vals, axis=1...  18.1 us
    psum x1, blocking collectives, per_device(): lax.psum((jnp.sum(norm_in, axis=1), jnp.sum(norm_in * centred, axis=1)),...  15.3 us
    psum x1, blocking collectives, per_device(): inner_sum = lax.psum(jnp.sum(gained * residual, axis=1), 'tp')  14.8 us
    all_to_all x1, blocking collectives, per_device(): lax.all_to_all(sent_inputs, 'sp', split_axis=0, concat_axis=0, tiled=True)  12.2 us
  transfers between devices with their start and end apart: 7, of which 6 were waited for; matrix products, arithmetic and copies ran while one was open for 8% of the time, Pallas kernels for 0%

commit v1 on v0

--- a/solution.py
+++ b/solution.py
@@ -1,9 +1,23 @@
+import functools
 import jax
 import jax.numpy as jnp
 from jax import lax
 from jax.sharding import PartitionSpec as P
 
 EPSILON = 1e-06
+
+
+def read_region_here(original, mesh_ax):
+    sides = []
+    for _ in range(lax.axis_size(mesh_ax)):
+        sides.append(original)
+    lower = jnp.stack(sides)
+    a_now = lax.all_to_all(lower, axis_name=mesh_ax, split_axis=0, concat_axis=0)
+    taken_in = jnp.concatenate(a_now, axis=1)
+    return taken_in
+
+
+packet_return_all = functools.partial(read_region_here, mesh_ax="tp")
 
 
 def shifted(block, axis, distance):
@@ -90,7 +104,7 @@
     )
     inputs, cotangent = (
         lax.all_gather(part_inputs.reshape(expert_rows, width_part), "tp", axis=1, tiled=True),
-        lax.all_gather(part_cotangent.reshape(expert_rows, width_part), "tp", axis=1, tiled=True),
+        packet_return_all(part_cotangent.reshape(expert_rows, width_part)),
     )
     gate_mat = w_gate[0]
     upper_mat = w_up[0]

time: 440 us -> 508 us (1.15)
  waiting for transfers between devices: 277 us -> 334 us
  starting transfers between devices: 5.63 us -> 12 us
    all_to_all x0 -> x1, waiting for transfers between devices: none -> 93.6 us  [read_region_here(): lax.all_to_all(lower, axis_name=mesh_ax, split_axis=0, concat_axis=0)]
    all_gather x1 -> x0, waiting for transfers between devices: 57.1 us -> none  [per_device(): lax.all_gather(part_cotangent.reshape(expert_rows, width_part), 'tp', axi...]
    all_gather x1, waiting for transfers between devices: 47.4 us -> 67.6 us  [per_device(): lax.all_gather(part_inputs.reshape(expert_rows, width_part), 'tp', axis=1...]
    all_to_all x0 -> x1, starting transfers between devices: none -> 6.44 us  [read_region_here(): lax.all_to_all(lower, axis_name=mesh_ax, split_axis=0, concat_axis=0)]
where the time goes in v1:
time: 508 us
  waiting for transfers between devices  334 us (66%)
  blocking collectives  72 us (14%)
  matrix products  48.6 us (10%)
  local copies, waits for them, and re-layouts  15.2 us (3%)
  between operations  14.1 us (3%)
  starting transfers between devices  12 us (2%)
  other arithmetic  11.8 us (2%)
    reduce_scatter x1, waiting for transfers between devices, per_device(): lax.psum_scatter(input_part, 'tp', scatter_dimension=1, tiled=True)  128 us
    all_to_all x1, waiting for transfers between devices, read_region_here(): lax.all_to_all(lower, axis_name=mesh_ax, split_axis=0, concat_axis=0)  93.6 us
    all_gather x1, waiting for transfers between devices, per_device(): lax.all_gather(part_inputs.reshape(expert_rows, width_part), 'tp', axis=1...  67.6 us
    all_gather x1, waiting for transfers between devices, per_device(): full_grad = lax.all_gather(stream_grad, 'tp', axis=1, tiled=True)  25.9 us
    psum x1, blocking collectives, per_device(): lax.psum((jnp.sum(residual * residual, axis=1), jnp.sum(conv_vals, axis=1...  18.1 us
    psum x1, blocking collectives, per_device(): lax.psum((jnp.sum(norm_in, axis=1), jnp.sum(norm_in * centred, axis=1)),...  15.3 us
    psum x1, blocking collectives, per_device(): inner_sum = lax.psum(jnp.sum(gained * residual, axis=1), 'tp')  14.8 us
    all_to_all x1, blocking collectives, per_device(): lax.all_to_all(sent_inputs, 'sp', split_axis=0, concat_axis=0, tiled=True)  12.2 us
  transfers between devices with their start and end apart: 7, of which 6 were waited for; matrix products, arithmetic and copies ran while one was open for 8% of the time, Pallas kernels for 0%

profile of v1, /device:TPU:0, one launch (start us, length us, event | category | flops | bytes accessed | tf_op | source)
XLA Modules:
  0.0 507.7 jit_solution(7902687879120564604)
XLA Ops:
  7.2 0.0 copy-start
  7.2 0.0 all-gather.3.cloned.1.call-start
  7.2 0.9 copy.39
  8.2 0.1 eq.60
  8.3 0.1 eq.56
  8.5 1.2 reduce-window.6
  9.7 0.2 slice_reduce_fusion
  9.9 0.2 reduce-window.9
  10.1 0.1 add_bitcast_fusion
  10.2 0.1 reduce_sum.85
  10.4 0.1 copy.41
  10.4 0.7 multiply_add_fusion
  11.1 0.2 fusion.22
  11.4 0.2 select_reduce_fusion
  11.6 1.1 fusion.15
  12.7 18.1 %psum.42 = f32[256]{0:T(256)S(1)} all-reduce(f32[256]{0:T(256)S(1)} %fusion.15), channel_id=1, replica_groups=mesh['sp'=4,'tp'=8] {'tp'}, use_global_device_ids=true, to_apply=%region_1.0 | all-reduce | flops 256 | bytes 2048 | tf_op jit(solution)/shard_map/psum | solution.py:62
  30.8 1.1 fusion.14
  31.9 0.0 copy-start.7
  31.9 2.7 gather_fusion
  34.6 12.2 %all_to_all.20 = bf16[4,192,512]{2,1,0:T(8,128)(2,1)} all-to-all(bf16[4,192,512]{2,1,0:T(8,128)(2,1)S(1)} %bitcast.101), channel_id=1, replica_groups=mesh['sp'=4,'tp'=8] {'sp'}, dimensions={0} | all-to-all | bytes 1572864 | tf_op jit(solution)/shard_map/all_to_all | solution.py:102
  46.8 0.0 all-gather.3.cloned.1.call-update
  46.8 2.7 gather_fusion.1
  49.5 0.2 add_reduce_fusion
  49.8 0.1 mul.483
  49.9 0.2 fusion.9
  50.1 11.7 %all_to_all.21 = bf16[4,192,512]{2,1,0:T(8,128)(2,1)} all-to-all(bf16[4,192,512]{2,1,0:T(8,128)(2,1)S(1)} %fusion.9), channel_id=1, replica_groups=mesh['sp'=4,'tp'=8] {'sp'}, dimensions={0} | all-to-all | bytes 1572864 | tf_op jit(solution)/shard_map/all_to_all | solution.py:103
  61.7 1.4 copy.42
  63.2 3.1 stack.3
  66.2 6.4 %all-to-all-start.2 = ((bf16[8,768,512]{1,2,0:T(8,128)(2,1)}), bf16[8,768,512]{1,2,0:T(8,128)(2,1)}, u32[]{:S(2)}, u32[]{:S(2)}) async-start(bf16[8,768,512]{1,2,0:T(8,128)(2,1)} %stack.3), calls=%async_computation.2 | async-start | bytes 12582912 | tf_op jit(solution)/shard_map/all_to_all | solution.py:15
  72.7 0.2 reduce-scatter.3.cloned.1.call-start
  72.9 67.6 %all-gather.3.cloned.1.call-done = bf16[768,4096]{1,0:T(8,128)(2,1)} async-done(((bf16[768,512]{1,0:T(8,128)(2,1)}), bf16[768,4096]{1,0:T(8,128)(2,1)}) %all-gather.3.cloned.1.call-update) | async-done | bytes 6291472 | tf_op jit(solution)/shard_map/all_gather | solution.py:106
  140.5 5.6 %fusion.2 = f32[768,256]{1,0:T(8,128)} fusion(bf16[768,4096]{1,0:T(8,128)(2,1)} %all-gather.3.cloned.1.call-done, bf16[1,4096,256]{2,1,0:T(8,128)(2,1)S(1)} %copy-done), kind=kOutput, calls=%fused_computation.37 | convolution fusion | flops 1610612736 | bytes 9175040 | tf_op jit(solution)/shard_map/dot_general | solution.py:112
  146.1 2.7 fusion.5
  148.8 93.6 %all-to-all-done.2 = bf16[8,768,512]{1,2,0:T(8,128)(2,1)} async-done(((bf16[8,768,512]{1,2,0:T(8,128)(2,1)}), bf16[8,768,512]{1,2,0:T(8,128)(2,1)}, u32[]{:S(2)}, u32[]{:S(2)}) %all-to-all-start.2) | async-done | bytes 6291488 | tf_op jit(solution)/shard_map/all_to_all | solution.py:15
  242.4 5.7 %multiply_convert_fusion.1 = (bf16[768,256]{1,0:T(8,128)(2,1)S(1)}, bf16[768,256]{1,0:T(8,128)(2,1)S(1)}) fusion(f32[768,256]{1,0:T(8,128)} %fusion.2, f32[768,256]{1,0:T(8,128)} %fusion.5, bf16[768,4096]{0,1:T(8,128)(2,1)} %bitcast.10, bf16[1,256,4096]{2,1,0:T(8,128)(2,1)} %param.21), kind=kOutput, calls=%fused_computation.54 | convolution fusion | flops 1613168640 | bytes 10747904 | tf_op jit(solution)/shard_map/dot_general | solution.py:115
  248.2 1.8 fusion
  250.0 6.6 %convolution_add_fusion = f32[768,4096]{1,0:T(8,128)} fusion(f32[768,4096]{1,0:T(8,128)S(1)} %fusion, bf16[768,256]{1,0:T(8,128)(2,1)S(1)} %get-tuple-element.47, bf16[1,4096,256]{2,1,0:T(8,128)(2,1)S(1)} %copy-done.5), kind=kOutput, calls=%fused_computation.2 | convolution fusion | flops 1613758464 | bytes 27656192 | tf_op jit(solution)/shard_map/dot_general | solution.py:131
  256.6 0.0 reduce-scatter.3.cloned.1.call-update
  256.7 127.8 %reduce-scatter.3.cloned.1.call-done = f32[768,512]{1,0:T(8,128)} async-done(((f32[768,4096]{1,0:T(8,128)}), f32[768,512]{1,0:T(8,128)}) %reduce-scatter.3.cloned.1.call-update) | async-done | bytes 1572880 | tf_op jit(solution)/shard_map/reduce_scatter | solution.py:134
  384.5 2.4 convert_element_type.72
  386.9 3.6 all-to-all-start.3
  390.5 0.1 convert_reduce_fusion
  390.7 8.9 %all-to-all-done.3 = bf16[4,192,512]{2,1,0:T(8,128)(2,1)S(1)} async-done(((bf16[4,192,512]{2,1,0:T(8,128)(2,1)}), bf16[4,192,512]{2,1,0:T(8,128)(2,1)S(1)}, u32[]{:S(2)}, u32[]{:S(2)}) %all-to-all-start.3) | async-done | bytes 786464 | tf_op jit(solution)/shard_map/all_to_all | solution.py:137
  399.6 0.5 fusion.20
  400.1 14.8 %all-reduce.3 = (f32[256]{0:T(256)S(1)}, f32[256]{0:T(256)S(1)}, f32[256]{0:T(256)S(1)}) all-reduce(f32[256]{0:T(256)S(1)} %get-tuple-element.88, f32[256]{0:T(256)S(1)} %get-tuple-element.39, f32[256]{0:T(256)S(1)} %get-tuple-element.38), channel_id=1, replica_groups=mesh['sp'=4,'tp'=8] {'tp'}, use_global_device_ids=true, to_apply=%region_10.11 | all-reduce | flops 768 | bytes 6144 | tf_op jit(solution)/shard_map/psum | solution.py:149
  414.9 0.9 fusion.19
  415.9 0.0 all-gather.5.cloned.1.call-update
  415.9 0.3 reduce-scatter.5.cloned.1.call-start
  416.2 25.9 %all-gather.5.cloned.1.call-done = bf16[256,4096]{1,0:T(8,128)(2,1)} async-done(((bf16[256,512]{1,0:T(8,128)(2,1)}), bf16[256,4096]{1,0:T(8,128)(2,1)}) %all-gather.5.cloned.1.call-update) | async-done | bytes 2097168 | tf_op jit(solution)/shard_map/all_gather | solution.py:152
  442.0 4.4 fusion.132
  446.4 0.0 reduce-scatter.5.cloned.1.call-update
  446.4 0.7 copy-done.12
  447.2 0.2 copy-done.10
  447.4 6.8 %convolution_bitcast_fusion.2 = f32[1,4096,256]{2,1,0:T(8,128)} fusion(bf16[768,4096]{1,0:T(8,128)(2,1)} %all-gather.3.cloned.1.call-done, bf16[768,256]{1,0:T(8,128)(2,1)S(1)} %copy-done.10), kind=kOutput, calls=%fused_computation.5 | convolution fusion | flops 1610612736 | bytes 10878976 | tf_op jit(solution)/shard_map/dot_general | solution.py:120
  454.2 6.9 %convolution_bitcast_fusion = f32[1,256,4096]{2,1,0:T(8,128)} fusion(bf16[768,4096]{0,1:T(8,128)(2,1)} %bitcast.10, f32[768,256]{1,0:T(8,128)S(1)} %copy-done.19, f32[768,256]{1,0:T(8,128)S(1)} %copy-done.18), kind=kOutput, calls=%fused_computation.3 | convolution fusion | flops 1611792384 | bytes 12058624 | tf_op jit(solution)/shard_map/dot_general | solution.py:126
  461.1 0.9 fusion.145
  461.9 15.3 %all-reduce.2 = (f32[256]{0:T(256)S(1)}, f32[256]{0:T(256)S(1)}) all-reduce(f32[256]{0:T(256)S(1)} %get-tuple-element.37, f32[256]{0:T(256)S(1)} %get-tuple-element.36), channel_id=1, replica_groups=mesh['sp'=4,'tp'=8] {'tp'}, use_global_device_ids=true, to_apply=%region_19.20 | all-reduce | flops 512 | bytes 4096 | tf_op jit(solution)/shard_map/psum | solution.py:173
  477.2 0.2 fusion.128
  477.5 1.4 collective-permute-start
  478.9 6.8 %convolution_bitcast_fusion.1 = f32[1,4096,256]{2,1,0:T(8,128)} fusion(bf16[768,4096]{1,0:T(8,128)(2,1)} %all-gather.3.cloned.1.call-done, bf16[768,256]{1,0:T(8,128)(2,1)S(1)} %get-tuple-element.47), kind=kOutput, calls=%fused_computation.4 | convolution fusion | flops 1610612736 | bytes 10878976 | tf_op jit(solution)/shard_map/dot_general | solution.py:123
  485.7 2.1 multiply_convert_fusion.4
  487.8 0.7 multiply_convert_fusion.5
  488.6 10.0 %reduce-scatter.5.cloned.1.call-done = f32[1024,256]{1,0:T(8,128)} async-done(((f32[4096,256]{1,0:T(8,128)}), f32[1024,256]{1,0:T(8,128)}) %reduce-scatter.5.cloned.1.call-update) | async-done | bytes 1048592 | tf_op jit(solution)/shard_map/reduce_scatter | solution.py:160
  498.6 2.5 copy.43
  (54 shorter events, 0.3 us)
Async XLA Ops:
  7.2 133.4 %copy-start = (bf16[1,4096,256]{2,1,0:T(8,128)(2,1)S(1)}, bf16[1,4096,256]{2,1,0:T(8,128)(2,1)}, u32[]{:S(2)}) copy-start(bf16[1,4096,256]{2,1,0:T(8,128)(2,1)} %param.19) | copy-start | bytes 6291460
  7.2 133.3 %all-gather.3.cloned.1.call-start = ((), (), s32[]{:S(2)}) async-start(), calls=%async_computation.6 | async-start | bytes 7077888 | tf_op jit(solution)/shard_map/all_gather | solution.py:106
  31.9 14.9 %copy-start.7 = (bf16[256,512]{1,0:T(8,128)(2,1)S(1)}, bf16[256,512]{1,0:T(8,128)(2,1)}, u32[]{:S(2)}) copy-start(bf16[256,512]{1,0:T(8,128)(2,1)} %param.14) | copy-start | bytes 786436
  46.8 2.8 copy-start.14
  66.2 176.2 %all-to-all-start.2 = ((bf16[8,768,512]{1,2,0:T(8,128)(2,1)}), bf16[8,768,512]{1,2,0:T(8,128)(2,1)}, u32[]{:S(2)}, u32[]{:S(2)}) async-start(bf16[8,768,512]{1,2,0:T(8,128)(2,1)} %stack.3), calls=%async_computation.2 | async-start | bytes 12582912 | tf_op jit(solution)/shard_map/all_to_all | solution.py:15
  72.7 311.8 %reduce-scatter.3.cloned.1.call-start = ((), (), s32[]{:S(2)}) async-start(), calls=%async_computation.7 | async-start | bytes 14155776 | tf_op jit(solution)/shard_map/reduce_scatter | solution.py:134
  140.5 5.6 %copy-start.4 = (bf16[1,4096,256]{2,1,0:T(8,128)(2,1)S(1)}, bf16[1,4096,256]{2,1,0:T(8,128)(2,1)}, u32[]{:S(2)}) copy-start(bf16[1,4096,256]{2,1,0:T(8,128)(2,1)} %param.20) | copy-start | bytes 6291460
  140.5 5.6 %copy-start.16 = (bf16[768,4096]{1,0:T(8,128)(2,1)S(1)}, bf16[768,4096]{1,0:T(8,128)(2,1)}, u32[]{:S(2)}) copy-start(bf16[768,4096]{1,0:T(8,128)(2,1)} %all-gather.3.cloned.1.call-done) | copy-start | bytes 18874372
  248.2 1.9 copy-start.9
  248.2 1.9 copy-start.5
  256.6 133.9 %copy-start.6 = (bf16[256,256]{1,0:T(8,128)(2,1)S(1)}, bf16[256,256]{1,0:T(8,128)(2,1)}, u32[]{:S(2)}) copy-start(bf16[256,256]{1,0:T(8,128)(2,1)} %param.24) | copy-start | bytes 393220
  256.6 143.0 %copy-start.3 = (bf16[256,512]{1,0:T(8,128)(2,1)S(1)}, bf16[256,512]{1,0:T(8,128)(2,1)}, u32[]{:S(2)}) copy-start(bf16[256,512]{1,0:T(8,128)(2,1)} %param.15) | copy-start | bytes 786436
  256.6 143.0 %copy-start.13 = (f32[512]{0:T(512)S(1)}, f32[512]{0:T(512)}, u32[]{:S(2)}) copy-start(f32[512]{0:T(512)} %param.16) | copy-start | bytes 6148
  256.7 185.4 %copy-start.15 = (f32[256]{0:T(256)S(1)}, f32[256]{0:T(256)}, u32[]{:S(2)}) copy-start(f32[256]{0:T(256)} %param.25) | copy-start | bytes 3076
  386.9 12.7 %all-to-all-start.3 = ((bf16[4,192,512]{2,1,0:T(8,128)(2,1)}), bf16[4,192,512]{2,1,0:T(8,128)(2,1)S(1)}, u32[]{:S(2)}, u32[]{:S(2)}) async-start(bf16[4,192,512]{2,1,0:T(8,128)(2,1)} %bitcast.18), calls=%async_computation.4 | async-start | bytes 1572864 | tf_op jit(solution)/shard_map/all_to_all | solution.py:137
  390.5 51.5 %all-gather.5.cloned.1.call-start = ((), (), s32[]{:S(2)}) async-start(), calls=%async_computation.8 | async-start | bytes 2359296 | tf_op jit(solution)/shard_map/all_gather | solution.py:152
  415.9 82.7 %reduce-scatter.5.cloned.1.call-start = ((), (), s32[]{:S(2)}) async-start(), calls=%async_computation.9 | async-start | bytes 5242880 | tf_op jit(solution)/shard_map/reduce_scatter | solution.py:160
  446.4 0.8 copy-start.12
  446.4 1.0 copy-start.10
  447.4 6.8 %copy-start.18 = (f32[768,256]{1,0:T(8,128)S(1)}, f32[768,256]{1,0:T(8,128)}, u32[]{:S(2)}) copy-start(f32[768,256]{1,0:T(8,128)} %fusion.2) | copy-start | bytes 2359300
  447.4 6.8 %copy-start.19 = (f32[768,256]{1,0:T(8,128)S(1)}, f32[768,256]{1,0:T(8,128)}, u32[]{:S(2)}) copy-start(f32[768,256]{1,0:T(8,128)} %fusion.5) | copy-start | bytes 2359300
  454.2 6.9 %copy-start.2 = (bf16[256,4096]{1,0:T(8,128)(2,1)S(1)}, bf16[256,4096]{1,0:T(8,128)(2,1)}, u32[]{:S(2)}) copy-start(bf16[256,4096]{1,0:T(8,128)(2,1)} %all-gather.5.cloned.1.call-done) | copy-start | bytes 6291460
  454.2 6.9 %copy-start.17 = (bf16[256,4096]{1,0:T(8,128)(2,1)S(1)}, bf16[256,4096]{1,0:T(8,128)(2,1)}, u32[]{:S(2)}) copy-start(bf16[256,4096]{1,0:T(8,128)(2,1)} %param.27) | copy-start | bytes 6291460
  477.5 8.3 %copy-start.8 = (bf16[256,256]{1,0:T(8,128)(2,1)S(1)}, bf16[256,256]{1,0:T(8,128)(2,1)}, u32[]{:S(2)}) copy-start(bf16[256,256]{1,0:T(8,128)(2,1)} %param.23) | copy-start | bytes 393220
  477.5 8.2 %copy-start.11 = (bf16[256,256]{1,0:T(8,128)(2,1)S(1)}, bf16[256,256]{1,0:T(8,128)(2,1)}, u32[]{:S(2)}) copy-start(bf16[256,256]{1,0:T(8,128)(2,1)} %param.22) | copy-start | bytes 393220
  477.5 8.2 %collective-permute-start = (f32[30,256]{1,0:T(8,128)S(1)}, f32[30,256]{1,0:T(8,128)S(1)}, u32[]{:S(2)}, u32[]{:S(2)}) collective-permute-start(f32[30,256]{1,0:T(8,128)S(1)} %slice.279), channel_id=1, source_target_pairs={{8,0},{16,8},{24,16},{9,1},{17,9},{25,17},{10,2},{18,10},{26,18},{... | collective-permute-start | bytes 92168 | tf_op jit(solution)/shard_map/ppermute | solution.py:26
  478.9 22.2 %copy-start.1 = (bf16[1,4096,256]{2,1,0:T(8,128)(2,1)S(1)}, bf16[1,4096,256]{2,1,0:T(8,128)(2,1)}, u32[]{:S(2)}) copy-start(bf16[1,4096,256]{2,1,0:T(8,128)(2,1)} %param.19) | copy-start | bytes 6291460
Sparse Core Ops, SparseCore 0:
  46.9 93.5 all-gather.2
  256.8 127.6 reduce-scatter.2
  416.0 25.9 all-gather.4
  446.6 51.9 reduce-scatter.4
